TPU v7x, 512 devices: a whole 4x4x16 slice. The times are simulated.
512 devices in a mesh: sp: 64 (over z, y), tp: 8 (over x, core).
Axes of the slice: x: 4, y: 4, z: 16, core: 2. Of those that a mesh axis runs over, the one named last changes fastest.
Arguments:
- tokens: bfloat16 [16384, 2048], P(('sp', 'tp')), may hold values from -96 to 96
- norm_gain: float32 [2048], replicated, may hold values from 0.1 to 1.9
- w_query: bfloat16 [2048, 1024], P(None, 'tp'), may hold values from -0.3 to 0.3
- w_key: bfloat16 [2048, 1024], P(None, 'tp'), may hold values from -0.3 to 0.3
- w_value: bfloat16 [2048, 1024], P(None, 'tp'), may hold values from -0.125 to 0.125
- w_att_gate: bfloat16 [2048, 1024], P(None, 'tp'), may hold values from -0.125 to 0.125
- w_rec_in: bfloat16 [2048, 1024], P(None, 'tp'), may hold values from -0.125 to 0.125
- w_rec_gate: bfloat16 [2048, 1024], P(None, 'tp'), may hold values from -0.125 to 0.125
- conv_taps: float32 [4, 1024], P(None, 'tp'), may hold values from -3 to 3
- gate_recur: bfloat16 [8, 128, 128], P('tp'), may hold values from -0.5 to 0.5
- gate_input: bfloat16 [8, 128, 128], P('tp'), may hold values from -0.5 to 0.5
- decay_rate: float32 [1024], P('tp'), may hold values from 1e-06 to 0.02
- head_lambda: float32 [8], P('tp'), may hold values from 0.3 to 0.8
- head_gain: float32 [1024], P('tp'), may hold values from 0.1 to 1.9
- out_att: bfloat16 [1024, 2048], P('tp'), may hold values from -0.125 to 0.125
- out_rec: bfloat16 [1024, 2048], P('tp'), may hold values from -0.125 to 0.125
Outputs:
- layer_out: bfloat16 [16384, 2048], P(('sp', 'tp'))
All inputs are finite; a program needn't handle non-finite values.
Results may differ from a plain program's by a relative error of at most 0.015.
Values may be sent and summed in bfloat16 or wider, within the bound.
A program may use at most 64 MiB of HBM per device.

v0:
```python
import math

import jax
import jax.numpy as jnp
from jax import lax
from jax.sharding import Mesh
from jax.sharding import PartitionSpec as P

SP = ("sp_0", "sp_1")
SP_TP = ("sp_0", "sp_1", "tp")


EPS_INPUT = 1e-06
EPS_HEAD = 1e-05
RATE_SCALE = 8.0
HEAD_FACTOR = 0.8
MASKED = -1e30


def side_by_side(arrays, axis, dim, along):
    ends, at = ([], 0)
    for a in arrays[:-1]:
        at += a.shape[along]
        ends.append(at)
    both = jnp.concatenate(arrays, axis=along)
    return tuple(jnp.split(lax.all_gather(both, axis, axis=dim, tiled=True), ends, axis=along))


def passed_along(block, axis, distance):
    devices = range(lax.axis_size(axis))
    route = [(i - distance, i) for i in devices if i - distance in devices]
    return lax.ppermute(block, axis, route)


def neutral_like(x, identity):
    return jax.tree.map(
        lambda part, zero: jnp.zeros_like(part) + jnp.asarray(zero, part.dtype), x, identity
    )


def gathered_once(x, axis):
    leaves = jax.tree.leaves(x)
    turns = sorted(range(len(leaves)), key=lambda k: -leaves[k].size)
    width = (1, *leaves[turns[0]].shape)[-1]
    lines = [
        jnp.pad(leaves[k].reshape(-1), (0, -leaves[k].size % width)).reshape(-1, width)
        for k in turns
    ]
    both, at, found = (lax.all_gather(jnp.concatenate(lines), axis), 0, {})
    for k, line in zip(turns, lines):
        piece = both[:, at : at + len(line)].reshape(len(both), -1)
        found[k] = piece[:, : leaves[k].size].reshape(-1, *leaves[k].shape)
        at += len(line)
    numbers = iter(range(len(leaves)))
    return jax.tree.map(lambda _: found[next(numbers)], x)


def entering(x, axes, combine, identity):
    before = start = neutral_like(x, identity)
    subtotal = x
    for axis in reversed(axes):
        devices, mine = (lax.axis_size(axis), lax.axis_index(axis))
        pieces = gathered_once(subtotal, axis)
        inside, subtotal = (start, start)
        for k in range(devices):
            passed = k < mine
            subtotal = combine(subtotal, jax.tree.map(lambda part: part[k], pieces))
            inside = jax.tree.map(lambda new, old: jnp.where(passed, new, old), subtotal, inside)
        before = combine(inside, before)
    return before


def copy_for_each(x, axis):
    devices = lax.axis_size(axis)
    return lax.all_to_all(jnp.broadcast_to(x[None], (devices, *x.shape)), axis, 0, 0, tiled=True)


def laid_out(blocks, dim):
    shape = list(blocks.shape[1:])
    shape[dim] *= blocks.shape[0]
    return jnp.moveaxis(blocks, 0, dim).reshape(shape)


def collect(x, axis, dim):
    blocks = copy_for_each(x, axis)
    return laid_out(blocks, dim)


def split_up(x, dim, devices):
    shape = x.shape
    blocks = x.reshape(*shape[:dim], devices, shape[dim] // devices, *shape[dim + 1 :])
    return jnp.moveaxis(blocks, dim, 0)


def summed_on_arrival(x, axis, dim):
    devices = lax.axis_size(axis)
    blocks = lax.all_to_all(split_up(x, dim, devices), axis, 0, 0, tiled=True)
    return jnp.sum(blocks.astype(jnp.float32), axis=0)


def rms_rows(values, gain, epsilon):
    mean_square = jnp.mean(values * values, axis=-1, keepdims=True)
    return values * lax.rsqrt(mean_square + epsilon) * gain


def combine_pair(earlier, later):
    return (earlier[0] * later[0], later[0] * earlier[1] + later[1])


def attention(queries, keys, values, head_lambda, head_gain, att_gate):
    rows = queries.shape[0]
    local_heads = head_lambda.shape[0]
    head_dim = queries.shape[1] // (2 * local_heads)
    value_dim = values.shape[1] // local_heads
    scale = head_dim ** (-0.5)
    query_heads = queries.reshape(rows, local_heads, 2, head_dim)
    query_pos = lax.axis_index(SP) * rows + jnp.arange(rows, dtype=jnp.int32)
    initial = (
        jnp.full((2, local_heads, rows), MASKED, jnp.float32),
        jnp.zeros((2, local_heads, rows), jnp.float32),
        jnp.zeros((2, local_heads, rows, value_dim), jnp.float32),
    )
    running = initial
    key_piece, value_piece = side_by_side((keys, values), SP, 0, 1)
    length = key_piece.shape[0]
    block_len = math.gcd(length, 512)
    block_count = length // block_len
    key_blocks = key_piece.reshape(block_count, block_len, local_heads, 2, head_dim)
    value_blocks = value_piece.reshape(block_count, block_len, local_heads, value_dim)
    block_starts = block_len * jnp.arange(block_count, dtype=jnp.int32)

    def one_block(current, inputs):
        key_block, value_block, block_start = inputs
        highest, totals, weighted = current
        key_pos = block_start + jnp.arange(block_len, dtype=jnp.int32)
        allowed = key_pos[None, :] <= query_pos[:, None]
        scores = (
            jnp.einsum(
                "qhpd,khpd->phqk", query_heads, key_block, preferred_element_type=jnp.float32
            )
            * scale
        )
        scores = jnp.where(allowed, scores, MASKED)
        new_high = jnp.maximum(highest, jnp.max(scores, axis=-1))
        factor = jnp.exp(highest - new_high)
        raised = jnp.where(allowed, jnp.exp(scores - new_high[..., None]), 0.0)
        totals = totals * factor + jnp.sum(raised, axis=-1)
        weighted = weighted * factor[..., None] + jnp.einsum(
            "phqk,khe->phqe",
            raised.astype(jnp.bfloat16),
            value_block,
            preferred_element_type=jnp.float32,
        )
        return ((new_high, totals, weighted), None)

    running, _ = lax.scan(one_block, running, (key_blocks, value_blocks, block_starts))
    highest, totals, weighted = running
    normalized = weighted / totals[..., None]
    per_head = normalized[0] - head_lambda[:, None, None] * normalized[1]
    head_out = (
        rms_rows(per_head, head_gain.reshape(local_heads, 1, value_dim), EPS_HEAD) * HEAD_FACTOR
    )
    head_out = jnp.moveaxis(head_out, 0, 1).reshape(rows, local_heads * value_dim)
    return (head_out * jax.nn.silu(att_gate.astype(jnp.float32))).astype(jnp.bfloat16)


def recurrence(rec_in, rec_gate, conv_taps, gate_recur, gate_input, decay_rate):
    rows, width = rec_in.shape
    taps = conv_taps.shape[0]
    earlier = passed_along(rec_in[rows - (taps - 1) :], SP, 1)
    padded = jnp.concatenate([earlier, rec_in], axis=0).astype(jnp.float32)
    conv_sum = jnp.zeros((rows, width), jnp.float32)
    for offset in range(taps):
        conv_sum = conv_sum + padded[offset : offset + rows] * conv_taps[offset]
    conv_out = conv_sum.astype(jnp.bfloat16)
    local_blocks = gate_recur.shape[0]
    grouped = conv_out.reshape(rows, local_blocks, gate_recur.shape[1])
    recur_gate = jax.nn.sigmoid(
        jnp.einsum("tnc,ncd->tnd", grouped, gate_recur, preferred_element_type=jnp.float32).reshape(
            rows, width
        )
    )
    inflow = jax.nn.sigmoid(
        jnp.einsum("tnc,ncd->tnd", grouped, gate_input, preferred_element_type=jnp.float32).reshape(
            rows, width
        )
    )
    log_decay = -RATE_SCALE * recur_gate * decay_rate
    decays = jnp.exp(log_decay)
    positions = lax.axis_index(SP) * rows + jnp.arange(rows, dtype=jnp.int32)
    norm_in = jnp.where((positions == 0)[:, None], 1.0, jnp.sqrt(-jnp.expm1(2.0 * log_decay)))
    driven = norm_in * inflow * conv_out.astype(jnp.float32)
    products, partial_states = lax.associative_scan(combine_pair, (decays, driven), axis=0)
    identity = (jnp.ones((width,), jnp.float32), jnp.zeros((width,), jnp.float32))
    incoming = entering((products[rows - 1], partial_states[rows - 1]), SP, combine_pair, identity)
    states = partial_states + products * incoming[1][None, :]
    return (states * jax.nn.silu(rec_gate.astype(jnp.float32))).astype(jnp.bfloat16)


def body(
    tokens,
    norm_gain,
    w_query,
    w_key,
    w_value,
    w_att_gate,
    w_rec_in,
    w_rec_gate,
    conv_taps,
    gate_recur,
    gate_input,
    decay_rate,
    head_lambda,
    head_gain,
    out_att,
    out_rec,
):
    normed = rms_rows(tokens.astype(jnp.float32), norm_gain, EPS_INPUT).astype(jnp.bfloat16)
    weights = (w_query, w_key, w_value, w_att_gate, w_rec_in, w_rec_gate)
    joined = jnp.concatenate(weights, axis=1)
    projected = jnp.dot(
        collect(normed, "tp", 0), joined, preferred_element_type=jnp.float32
    ).astype(jnp.bfloat16)
    bounds = [0]
    for weight in weights:
        bounds.append(bounds[-1] + weight.shape[1])
    queries, keys, values, att_gate, rec_in, rec_gate = [
        projected[:, bounds[index] : bounds[index + 1]] for index in range(6)
    ]
    att_mixed = attention(queries, keys, values, head_lambda, head_gain, att_gate)
    rec_mixed = recurrence(rec_in, rec_gate, conv_taps, gate_recur, gate_input, decay_rate)
    total = summed_on_arrival(
        (
            jnp.dot(att_mixed, out_att, preferred_element_type=jnp.float32)
            + jnp.dot(rec_mixed, out_rec, preferred_element_type=jnp.float32)
        ).astype(jnp.bfloat16),
        "tp",
        0,
    )
    return total.astype(jnp.bfloat16)


def solution(mesh):
    finer = Mesh(mesh.devices.reshape(16, 4, mesh.shape["tp"]), ("sp_0", "sp_1", "tp"))
    placed = (
        P(SP_TP, None),
        P(),
        P(None, "tp"),
        P(None, "tp"),
        P(None, "tp"),
        P(None, "tp"),
        P(None, "tp"),
        P(None, "tp"),
        P(None, "tp"),
        P("tp", None, None),
        P("tp", None, None),
        P("tp"),
        P("tp"),
        P("tp"),
        P("tp", None),
        P("tp", None),
    )
    return jax.shard_map(
        body, mesh=finer, in_specs=placed, out_specs=P(SP_TP, None), check_vma=False
    )
```

profile of v0, /device:TPU:1, one launch (start us, length us, event | category | flops | bytes accessed | tf_op | source)
XLA Modules:
  0.0 397.5 jit_solution(6756415968171534123)
XLA Ops:
  9.8 10.3 %all-to-all-start = ((bf16[8,32,2048]{2,1,0:T(8,128)(2,1)}), bf16[8,32,2048]{2,1,0:T(8,128)(2,1)S(1)}, u32[]{:S(2)}, u32[]{:S(2)}) async-start(bf16[8,32,2048]{2,1,0:T(8,128)(2,1)} %broadcast_in_dim.62), calls=%async_computation | async-start | bytes 2097152 | tf_op jit(solution)/shard_map/all_to_all | solution.py:75
  25.5 9.6 %all-to-all-done = bf16[8,32,2048]{2,1,0:T(8,128)(2,1)S(1)} async-done(((bf16[8,32,2048]{2,1,0:T(8,128)(2,1)}), bf16[8,32,2048]{2,1,0:T(8,128)(2,1)S(1)}, u32[]{:S(2)}, u32[]{:S(2)}) %all-to-all-start) | async-done | bytes 1048608 | tf_op jit(solution)/shard_map/all_to_all | solution.py:75
  35.1 2.9 convolution_convert_fusion
  39.5 1.3 collective-permute-start
  44.0 6.9 %all-gather.2 = f32[4,2,128]{2,1,0:T(2,128)S(1)} all-gather(f32[1,2,128]{2,1,0:T(2,128)S(1)} %maximum_bitcast_fusion), channel_id=2, replica_groups=mesh['sp_0'=16,'sp_1'=4,'tp'=8] {'sp_1'}, dimensions={0}, use_global_device_ids=true | all-gather | bytes 5120 | tf_op jit(solution)/shard_map/all_gather | solution.py:49
  50.9 28.2 %all-gather.3 = f32[16,2,128]{2,1,0:T(2,128)S(1)} all-gather(f32[1,2,128]{2,1,0:T(2,128)S(1)} %maximum_bitcast_fusion.1), channel_id=3, replica_groups=mesh['sp_0'=16,'sp_1'=4,'tp'=8] {'sp_0'}, dimensions={0}, use_global_device_ids=true | all-gather | bytes 17408 | tf_op jit(solution)/shard_map/all_gather | solution.py:49
  79.2 106.4 %all-gather.6.cloned.1.call-done = bf16[16384,256]{1,0:T(8,128)(2,1)} async-done(((bf16[256,256]{1,0:T(8,128)(2,1)}), bf16[16384,256]{1,0:T(8,128)(2,1)}) %all-gather.6.cloned.1.call-update) | async-done | bytes 8388624 | tf_op jit(solution)/shard_map/all_gather | solution.py:26
  185.6 5.7 %fusion.95 = (bf16[16384,128]{1,0:T(8,128)(2,1)}, bf16[16384,128]{1,0:T(8,128)(2,1)}) fusion(bf16[16384,256]{1,0:T(8,128)(2,1)} %all-gather.6.cloned.1.call-done), kind=kLoop, calls=%fused_computation.252 | loop fusion | bytes 16777216 | tf_op jit(solution)/shard_map/split | solution.py:26
  191.3 14.8 %reshape.637 = bf16[32,512,1,2,64]{4,3,1,0,2:T(2,128)(2,1)} reshape(bf16[16384,128]{1,0:T(8,128)(2,1)} %get-tuple-element.138) | data formatting | bytes 8388608 | tf_op jit(solution)/shard_map/reshape | solution.py:128
  206.1 18.4 %copy.31 = bf16[32,512,1,2,64]{1,4,3,2,0:T(8,128)(2,1)} copy(bf16[32,512,1,2,64]{4,3,1,0,2:T(2,128)(2,1)} %reshape.637) | data formatting | bytes 8388608
  224.4 136.5 %while.15 = (s32[]{:T(128)}, f32[2,1,256]{2,0,1:T(2,128)S(1)}, f32[2,1,256]{2,0,1:T(2,128)S(1)}, f32[2,1,256,128]{2,3,0,1:T(8,128)S(1)}, s32[32]{0:T(128)S(1)}, ...) while((s32[]{:T(128)}, f32[2,1,256]{2,0,1:T(2,128)S(1)}, ...), condition=%wide.region_4.5_spmd.clone, body=%wide.region_1.4_spmd.clone.sunk | while | flops 103354112 | bytes 4561053 | solution.py:156
  227.4 1.3 fusion.116
  231.7 1.3 fusion.116
  235.9 1.3 fusion.116
  240.2 1.3 fusion.116
  244.4 1.3 fusion.116
  248.7 1.3 fusion.116
  253.0 1.3 fusion.116
  257.2 1.3 fusion.116
  261.5 1.3 fusion.116
  265.8 1.3 fusion.116
  270.0 1.3 fusion.116
  274.3 1.3 fusion.116
  278.6 1.3 fusion.116
  282.8 1.3 fusion.116
  295.6 1.3 fusion.116
  304.2 1.3 fusion.116
  308.4 1.3 fusion.116
  317.0 1.3 fusion.116
  346.8 1.3 fusion.116
  355.3 1.3 fusion.116
  362.4 27.4 %all_to_all.10 = bf16[8,32,2048]{2,1,0:T(8,128)(2,1)S(1)} all-to-all(bf16[8,32,2048]{2,1,0:T(8,128)(2,1)S(1)} %bitcast.291), channel_id=1, replica_groups=mesh['sp_0'=16,'sp_1'=4,'tp'=8] {'tp'}, dimensions={0} | all-to-all | bytes 2097152 | tf_op jit(solution)/shard_map/all_to_all | solution.py:97
  (489 shorter events, 122.5 us)
Async XLA Ops:
  6.5 354.8 %copy-start = (bf16[128,2048]{1,0:T(8,128)(2,1)S(1)}, bf16[128,2048]{1,0:T(8,128)(2,1)}, u32[]{:S(2)}) copy-start(bf16[128,2048]{1,0:T(8,128)(2,1)} %param.32) | copy-start | bytes 1572868
  6.5 13.6 %copy-start.2 = (bf16[2048,128]{1,0:T(8,128)(2,1)S(1)}, bf16[2048,128]{1,0:T(8,128)(2,1)}, u32[]{:S(2)}) copy-start(bf16[2048,128]{1,0:T(8,128)(2,1)} %param.20) | copy-start | bytes 1572868
  6.5 14.5 %copy-start.3 = (bf16[2048,128]{1,0:T(8,128)(2,1)S(1)}, bf16[2048,128]{1,0:T(8,128)(2,1)}, u32[]{:S(2)}) copy-start(bf16[2048,128]{1,0:T(8,128)(2,1)} %param.21) | copy-start | bytes 1572868
  6.5 15.4 %copy-start.4 = (bf16[2048,128]{1,0:T(8,128)(2,1)S(1)}, bf16[2048,128]{1,0:T(8,128)(2,1)}, u32[]{:S(2)}) copy-start(bf16[2048,128]{1,0:T(8,128)(2,1)} %param.22) | copy-start | bytes 1572868
  9.8 25.3 %all-to-all-start = ((bf16[8,32,2048]{2,1,0:T(8,128)(2,1)}), bf16[8,32,2048]{2,1,0:T(8,128)(2,1)S(1)}, u32[]{:S(2)}, u32[]{:S(2)}) async-start(bf16[8,32,2048]{2,1,0:T(8,128)(2,1)} %broadcast_in_dim.62), calls=%async_computation | async-start | bytes 2097152 | tf_op jit(solution)/shard_map/all_to_all | solution.py:75
  20.1 165.5 %all-gather.6.cloned.1.call-start = ((), (), s32[]{:S(2)}) async-start(), calls=%async_computation.2 | async-start | bytes 8519680 | tf_op jit(solution)/shard_map/all_gather | solution.py:26
  20.1 2.7 copy-start.5
  20.2 3.6 copy-start.6
  20.2 4.4 %copy-start.7 = (bf16[2048,128]{1,0:T(8,128)(2,1)S(1)}, bf16[2048,128]{1,0:T(8,128)(2,1)}, u32[]{:S(2)}) copy-start(bf16[2048,128]{1,0:T(8,128)(2,1)} %param.25) | copy-start | bytes 1572868
  25.5 14.0 %copy-start.12 = (f32[128]{0:T(128)S(1)}, f32[128]{0:T(128)}, u32[]{:S(2)}) copy-start(f32[128]{0:T(128)} %param.29) | copy-start | bytes 1540
  25.5 14.0 %copy-start.8 = (f32[4,128]{1,0:T(4,128)S(1)}, f32[4,128]{1,0:T(4,128)}, u32[]{:S(2)}) copy-start(f32[4,128]{1,0:T(4,128)} %param.26) | copy-start | bytes 6148
  35.1 6.5 %copy-start.10 = (bf16[1,128,128]{2,1,0:T(8,128)(2,1)S(1)}, bf16[1,128,128]{2,1,0:T(8,128)(2,1)}, u32[]{:S(2)}) copy-start(bf16[1,128,128]{2,1,0:T(8,128)(2,1)} %param.27) | copy-start | bytes 98308
  35.1 6.7 %copy-start.11 = (bf16[1,128,128]{2,1,0:T(8,128)(2,1)S(1)}, bf16[1,128,128]{2,1,0:T(8,128)(2,1)}, u32[]{:S(2)}) copy-start(bf16[1,128,128]{2,1,0:T(8,128)(2,1)} %param.28) | copy-start | bytes 98308
  39.5 2.0 collective-permute-start
  224.4 136.9 %copy-start.9 = (f32[128]{0:T(128)S(1)}, f32[128]{0:T(128)}, u32[]{:S(2)}) copy-start(f32[128]{0:T(128)} %param.31) | copy-start | bytes 1540
  360.9 1.0 copy-start.1
Sparse Core Ops, SparseCore 0:
  38.8 146.7 all-gather.5
where the time goes:
time: 400 us; the launch traced here: 397 us
  waiting for transfers between devices  117 us (29%)
  matrix products  85.9 us (21%)
  local copies, waits for them, and re-layouts  66.1 us (17%)
  blocking collectives  62.6 us (16%)
  other arithmetic  37.4 us (9%)
  between operations  15 us (4%)
  starting transfers between devices  11.6 us (3%)
    all_gather x1, waiting for transfers between devices, side_by_side(): lax.all_gather(both, axis, axis=dim, tiled=True)  106 us
    dot_general x32, matrix products, one_block(): jnp.einsum('phqk,khe->phqe', raised.astype(jnp.bfloat16), value_block, pr...  41.1 us
    dot_general x32, matrix products, one_block(): jnp.einsum('qhpd,khpd->phqk', query_heads, key_block, preferred_element_t...  40.6 us
    all_gather x2, blocking collectives, gathered_once(): both, at, found = (lax.all_gather(jnp.concatenate(lines), axis), 0, {})  35.2 us
    all_to_all x1, blocking collectives, summed_on_arrival(): blocks = lax.all_to_all(split_up(x, dim, devices), axis, 0, 0, tiled=True)  27.4 us
    unnamed x32, local copies, waits for them, and re-layouts  23 us
    add x32, other arithmetic, one_block(): key_pos = block_start + jnp.arange(block_len, dtype=jnp.int32)  20.7 us
    dynamic_slice x32, local copies, waits for them, and re-layouts, attention(): lax.scan(one_block, running, (key_blocks, value_blocks, block_starts))  18.8 us
  transfers between devices with their start and end apart: 3, of which 3 were waited for; matrix products, arithmetic and copies ran while one was open for 2% of the time, Pallas kernels for 0%

commit v1 on v0

v1 whole, which is shorter than its diff:
```python
import functools
import math

import jax
import jax.numpy as jnp
from jax import lax
from jax.experimental import pallas as pl
from jax.experimental.pallas import tpu as pltpu
from jax.sharding import PartitionSpec as P

MESH = pl.DeviceIdType.MESH
F32 = jnp.float32
BF16 = jnp.bfloat16

EPS_INPUT = 1e-06
EPS_HEAD = 1e-05
RATE_SCALE = 8.0
HEAD_FACTOR = 0.8
MASKED = -1e30
LOG2E = math.log2(math.e)
WIDTH = 128


def minus_expm1(x):
    series = 1.0 + x * (
        1 / 2 + x * (1 / 6 + x * (1 / 24 + x * (1 / 120 + x * (1 / 720 + x * (1 / 5040)))))
    )
    return jnp.where(x > -0.5, -x * series, 1.0 - jnp.exp(x))


def kernel(
    Z, Y, X,
    tokens, norm_gain, w_query, w_key, w_value, w_att_gate, w_rec_in, w_rec_gate, conv_taps,
    gate_recur, gate_input, decay_rate, head_lambda, head_gain, out_att, out_rec,
    out,
    wcat, wout, xbuf, kbuf, vbuf, qbuf, qext, acc, m_ref, l_ref, gate_s, rec_s, recg_s, halo, ext,
    prods, parts, yagg, zagg, stat, cbuf, pbuf, own_c, mixed, ptx, prx, own_o, rtx, rrx,
    w_sem, ag_s, ag_r, kv_s, kv_r, q_s, q_r, halo_s, halo_r, ya_s, ya_r, za_s, za_r,
    st_s, st_r, cb_s, cb_r, pr_s, pr_r, rs_s, rs_r,
):
    rows = tokens.shape[0]
    R = xbuf.shape[0]
    H, G = Z // 2, Z - 1 - Z // 2
    sp, tp = lax.axis_index("sp"), lax.axis_index("tp")
    z, y = sp // Y, sp % Y
    x, c = tp // 2, tp % 2
    way = 1 - 2 * c
    x_fwd, x_bwd, x_far = (x + way + X) % X, (x - way + X) % X, (x + 2) % X
    partner = (sp, 2 * x + 1 - c)
    fwd, bwd = (sp, 2 * x_fwd + c), (sp, 2 * x_bwd + c)
    z_up, z_down = (((z + 1) % Z) * Y + y, tp), (((z + Z - 1) % Z) * Y + y, tp)
    sp_next, sp_prev = ((sp + 1) % (Z * Y), tp), ((sp + Z * Y - 1) % (Z * Y), tp)

    def plane(d):
        return (z * Y + (y + d) % Y, tp)

    def remote(src, dst, send, recv, device):
        return pltpu.make_async_remote_copy(
            src_ref=src, dst_ref=dst, send_sem=send, recv_sem=recv,
            device_id=device, device_id_type=MESH,
        )

    loads = [
        pltpu.make_async_copy(w, wcat.at[:, i * WIDTH : (i + 1) * WIDTH], w_sem.at[i])
        for i, w in enumerate((w_key, w_value, w_query, w_att_gate, w_rec_in, w_rec_gate))
    ]
    loads += [
        pltpu.make_async_copy(w, wout.at[i * WIDTH : (i + 1) * WIDTH, :], w_sem.at[6 + i])
        for i, w in enumerate((out_att, out_rec))
    ]
    for load in loads:
        load.start()

    barrier = pltpu.get_barrier_semaphore()
    peers = [partner, fwd, bwd, z_up, z_down, sp_next, sp_prev] + [plane(d) for d in range(1, Y)]
    for peer in peers:
        pl.semaphore_signal(barrier, inc=1, device_id=peer, device_id_type=MESH)

    tok = tokens[...].astype(F32)
    scale = lax.rsqrt(jnp.mean(tok * tok, axis=-1, keepdims=True) + EPS_INPUT)
    xbuf[pl.ds(pl.multiple_of(tp * rows, rows), rows), :] = (tok * scale * norm_gain[...]).astype(BF16)

    pl.semaphore_wait(barrier, len(peers))

    def ag(slot, device, k):
        piece = xbuf.at[pl.ds(pl.multiple_of(slot * rows, rows), rows), :]
        return remote(piece, piece, ag_s.at[k], ag_r.at[slot], device)

    sent = []

    def send(copy):
        copy.start()
        sent.append(copy)

    send(ag(tp, fwd, 0))
    send(ag(tp, bwd, 1))
    send(ag(tp, partner, 2))
    ag(2 * x_bwd + c, fwd, 3).wait_recv()
    send(ag(2 * x_bwd + c, fwd, 3))
    send(ag(2 * x_bwd + c, partner, 4))
    ag(2 * x_fwd + c, partner, 5).wait_recv()
    send(ag(2 * x_fwd + c, partner, 5))
    ag(2 * x_far + c, partner, 6).wait_recv()
    send(ag(2 * x_far + c, partner, 6))
    for i in range(X):
        ag(2 * i + 1 - c, partner, 6).wait_recv()

    for load in loads[:2]:
        load.wait()
    normed = xbuf[...]
    kv = jnp.dot(normed, wcat[:, : 2 * WIDTH], preferred_element_type=F32)
    kbuf[z] = kv[:, :WIDTH].astype(BF16)
    vbuf[z] = kv[:, WIDTH:].T.astype(BF16)

    bufs = (kbuf, vbuf)

    def ring(way_, kind, slot, step):
        piece = bufs[kind].at[slot]
        return remote(
            piece, piece, kv_s.at[2 * way_ + kind, step], kv_r.at[kind, slot],
            (z_up, z_down)[way_],
        )

    for kind in range(2):
        ring(0, kind, z, 0).start()
        if G > 0:
            ring(1, kind, z, 0).start()

    for load in loads[2:4]:
        load.wait()
    qg = jnp.dot(normed, wcat[:, 2 * WIDTH : 4 * WIDTH], preferred_element_type=F32)
    qbuf[y] = qg[:, :WIDTH].T.astype(BF16)
    for d in range(1, Y):
        send(remote(qbuf.at[y], qbuf.at[y], q_s.at[d], q_r.at[y], plane(d)))
    gate_s[...] = qg[:, WIDTH:].astype(BF16)

    for load in loads[4:]:
        load.wait()
    rr = jnp.dot(normed, wcat[:, 4 * WIDTH :], preferred_element_type=F32)
    rec_s[...] = rr[:, :WIDTH].astype(BF16)
    send(remote(rec_s.at[R - 16 :, :], halo, halo_s, halo_r, sp_next))
    recg_s[...] = rr[:, WIDTH:].astype(BF16)

    row = lax.broadcasted_iota(jnp.int32, (R, WIDTH), 0)

    remote(halo, halo, halo_s, halo_r, sp_next).wait_recv()
    ext[0:16, :] = jnp.where(sp > 0, halo[...].astype(F32), 0.0)
    ext[16:, :] = rec_s[...].astype(F32)
    conv = jnp.zeros((R, WIDTH), F32)
    for j in range(4):
        conv = conv + ext[13 + j : 13 + j + R, :] * conv_taps[j : j + 1, :]
    conv_out = conv.astype(BF16)
    recur = jax.nn.sigmoid(jnp.dot(conv_out, gate_recur[0], preferred_element_type=F32))
    inflow = jax.nn.sigmoid(jnp.dot(conv_out, gate_input[0], preferred_element_type=F32))
    log_decay = -RATE_SCALE * recur * decay_rate[...]
    first = jnp.logical_and(row == 0, sp == 0)
    factor = jnp.where(first, 1.0, jnp.sqrt(minus_expm1(2.0 * log_decay)))
    a = jnp.exp(log_decay)
    b = factor * inflow * conv_out.astype(F32)
    k = 1
    while k < R:
        inside = row >= k
        b = b + a * jnp.where(inside, pltpu.roll(b, k, 0), 0.0)
        a = a * jnp.where(inside, pltpu.roll(a, k, 0), 1.0)
        k *= 2
    prods[...] = a
    parts[...] = b
    sub = lax.broadcasted_iota(jnp.int32, (8, WIDTH), 0)
    yagg[y] = jnp.where(sub == 0, a[R - 1 : R, :], b[R - 1 : R, :])
    for d in range(1, Y):
        send(remote(yagg.at[y], yagg.at[y], ya_s.at[d], ya_r.at[y], plane(d)))

    def plane_total():
        for d in range(1, Y):
            src = (y + d) % Y
            remote(yagg.at[src], yagg.at[src], ya_s.at[0], ya_r.at[src], plane(d)).wait_recv()
        ta, tb = yagg[0, 0:1, :], yagg[0, 1:2, :]
        for i in range(1, Y):
            ia, ib = yagg[i, 0:1, :], yagg[i, 1:2, :]
            ta, tb = ia * ta, ia * tb + ib
        zagg[z] = jnp.where(sub == 0, ta, tb)
        state(0, z, 0).start()
        if G > 0:
            state(1, z, 0).start()

    def state(way_, slot, step):
        piece = zagg.at[slot]
        return remote(piece, piece, za_s.at[way_, step], za_r.at[slot], (z_up, z_down)[way_])

    def state_step(j):
        up, down = (z - j + Z) % Z, (z + j) % Z
        state(0, up, 0).wait_recv()

        @pl.when(j < H)
        def _():
            state(0, up, j).start()

        @pl.when(j <= G)
        def _():
            state(1, down, 0).wait_recv()

            @pl.when(j < G)
            def _():
                state(1, down, j).start()

    def tile(slot, opening):
        key = kbuf[slot]
        keys = jnp.concatenate([key, key], axis=1)
        value = vbuf[slot]
        for i in range(2 * Y):
            s = jnp.dot(keys, qext[i], preferred_element_type=F32)
            if opening:
                pos = lax.broadcasted_iota(jnp.int32, (R, R), 1) - lax.broadcasted_iota(
                    jnp.int32, (R, R), 0
                )
                allowed = pos + (i // 2 - y) * R >= 0
                s = jnp.where(allowed, s, MASKED)
                top = jnp.max(s, axis=0, keepdims=True)
                p = jnp.where(allowed, jnp.exp2(s - top), 0.0)
                l_ref[i : i + 1, :] = jnp.sum(p, axis=0, keepdims=True)
                acc[i] = jnp.dot(value, p.astype(BF16), preferred_element_type=F32)
            else:
                old = m_ref[i : i + 1, :]
                top = jnp.maximum(old, jnp.max(s, axis=0, keepdims=True))
                p = jnp.exp2(s - top)
                fade = jnp.exp2(old - top)
                l_ref[i : i + 1, :] = l_ref[i : i + 1, :] * fade + jnp.sum(p, axis=0, keepdims=True)
                acc[i] = acc[i] * fade + jnp.dot(value, p.astype(BF16), preferred_element_type=F32)
            m_ref[i : i + 1, :] = top

    def opening():
        for d in range(1, Y):
            src = (y + d) % Y
            remote(qbuf.at[src], qbuf.at[src], q_s.at[0], q_r.at[src], plane(d)).wait_recv()
        half = WIDTH // 2
        none = jnp.zeros((half, R), BF16)
        for i in range(Y):
            q = qbuf[i].astype(F32) * (LOG2E * half ** -0.5)
            high = q.astype(BF16)
            low = (q - high.astype(F32)).astype(BF16)
            qext[2 * i] = jnp.concatenate([high[:half], none, low[:half], none], axis=0)
            qext[2 * i + 1] = jnp.concatenate([none, high[half:], none, low[half:]], axis=0)
        tile(z, True)

    def step(s, carry):
        up, down = (z - s + Z) % Z, (z + s) % Z
        for kind in range(2):
            ring(0, kind, up, 0).wait_recv()

            @pl.when(s < H)
            def _():
                ring(0, kind, up, s).start()

            @pl.when(s <= G)
            def _():
                ring(1, kind, down, 0).wait_recv()

                @pl.when(s < G)
                def _():
                    ring(1, kind, down, s).start()

        @pl.when(s == 1)
        def _():
            opening()

        @pl.when(s == 2)
        def _():
            plane_total()

        @pl.when(s > 2)
        def _():
            state_step(s - 2)

        @pl.when(z >= s)
        def _():
            tile(up, False)

        @pl.when(jnp.logical_and(s <= G, z + s >= Z))
        def _():
            tile(down, False)

        return carry

    lax.fori_loop(1, H + 1, step, 0)

    stat[y, 0 : 2 * Y, :] = m_ref[0 : 2 * Y, :]
    stat[y, 2 * Y : 4 * Y, :] = l_ref[0 : 2 * Y, :]
    for d in range(1, Y):
        send(remote(stat.at[y], stat.at[y], st_s.at[d], st_r.at[y], plane(d)))
    for d in range(1, Y):
        src = (y + d) % Y
        remote(stat.at[src], stat.at[src], st_s.at[0], st_r.at[src], plane(d)).wait_recv()
    lam = head_lambda[...]

    def comb_copy(i):
        return remote(cbuf.at[i], pbuf.at[y], cb_s.at[i], cb_r.at[y], (z * Y + i, tp))

    for i in range(Y):
        weight = []
        for n in (2 * i, 2 * i + 1):
            tops = [stat[j, n : n + 1, :] for j in range(Y)]
            top = functools.reduce(jnp.maximum, tops)
            total = sum(stat[j, 2 * Y + n : 2 * Y + n + 1, :] * jnp.exp2(tops[j] - top) for j in range(Y))
            weight.append(jnp.exp2(m_ref[n : n + 1, :] - top) / total)
        comb = acc[2 * i] * weight[0] - acc[2 * i + 1] * (weight[1] * lam)

        @pl.when(y == i)
        def _():
            own_c[...] = comb

        @pl.when(y != i)
        def _():
            cbuf[i] = comb.astype(BF16)
            comb_copy(i).start()

    def late(j, carry):
        state_step(j)
        return carry

    lax.fori_loop(max(H - 1, 1), H + 1, late, 0)
    h = jnp.zeros((1, WIDTH), F32)
    for i in range(Z - 1):
        h = jnp.where(i < z, zagg[i, 0:1, :] * h + zagg[i, 1:2, :], h)
    for i in range(Y - 1):
        h = jnp.where(i < y, yagg[i, 0:1, :] * h + yagg[i, 1:2, :], h)
    states = parts[...] + prods[...] * h
    recg = recg_s[...].astype(F32)
    mixed[:, WIDTH:] = (states * (recg * jax.nn.sigmoid(recg))).astype(BF16)

    total = own_c[...]
    for d in range(1, Y):
        src = (y + d) % Y
        remote(pbuf.at[src], pbuf.at[src], cb_s.at[0], cb_r.at[src], plane(d)).wait_recv()
        total = total + pbuf[src].astype(F32)
    total = total * lax.rsqrt(jnp.mean(total * total, axis=0, keepdims=True) + EPS_HEAD)
    gate = gate_s[...].astype(F32)
    att = total.T * head_gain[...] * HEAD_FACTOR * (gate * jax.nn.sigmoid(gate))
    mixed[:, :WIDTH] = att.astype(BF16)

    def group(core):
        return jnp.concatenate(
            [
                mixed[pl.ds(pl.multiple_of((2 * i + core) * rows, rows), rows), :]
                for i in range(X)
            ],
            axis=0,
        )

    wo = wout[...]
    ptx[...] = jnp.dot(group(1 - c), wo, preferred_element_type=F32).astype(BF16).reshape(ptx.shape)
    send(remote(ptx, prx, pr_s, pr_r, partner))
    own_o[...] = jnp.dot(group(c), wo, preferred_element_type=F32).reshape(own_o.shape)
    remote(ptx, prx, pr_s, pr_r, partner).wait_recv()

    def both(i):
        return own_o[i] + prx[i].astype(F32)

    def hop(k, device):
        return remote(rtx.at[k], rrx.at[k], rs_s.at[k], rs_r.at[k], device)

    rtx[0] = both(x_far).astype(BF16)
    send(hop(0, fwd))
    rtx[1] = both(x_bwd).astype(BF16)
    send(hop(1, bwd))
    hop(0, fwd).wait_recv()
    rtx[2] = (both(x_fwd) + rrx[0].astype(F32)).astype(BF16)
    send(hop(2, fwd))
    hop(1, bwd).wait_recv()
    mine = both(x) + rrx[1].astype(F32)
    hop(2, fwd).wait_recv()
    out[...] = (mine + rrx[2].astype(F32)).astype(BF16)

    for copy in sent:
        copy.wait_send()
    for i in range(Y):

        @pl.when(y != i)
        def _():
            comb_copy(i).wait_send()

    def drain(s, carry):
        for kind in range(2):
            ring(0, kind, z, s).wait_send()

            @pl.when(s < G)
            def _():
                ring(1, kind, z, s).wait_send()

        state(0, z, s).wait_send()

        @pl.when(s < G)
        def _():
            state(1, z, s).wait_send()

        return carry

    lax.fori_loop(0, H, drain, 0)


def build(mesh, Y):
    SP, TP = mesh.shape["sp"], mesh.shape["tp"]
    Z, X = SP // Y, TP // 2

    def body(
        tokens, norm_gain, w_query, w_key, w_value, w_att_gate, w_rec_in, w_rec_gate, conv_taps,
        gate_recur, gate_input, decay_rate, head_lambda, head_gain, out_att, out_rec,
    ):
        rows, D = tokens.shape
        R = rows * TP
        H, G = Z // 2, max(Z - 1 - Z // 2, 1)
        vmem, far = pl.BlockSpec(memory_space=pltpu.VMEM), pl.BlockSpec(memory_space=pl.ANY)
        V, dma = pltpu.VMEM, pltpu.SemaphoreType.DMA
        scratch = [
            V((D, 6 * WIDTH), BF16), V((2 * WIDTH, D), BF16), V((R, D), BF16),
            V((Z, R, WIDTH), BF16), V((Z, WIDTH, R), BF16), V((Y, WIDTH, R), BF16),
            V((2 * Y, 2 * WIDTH, R), BF16), V((2 * Y, WIDTH, R), F32),
            V((2 * Y, R), F32), V((2 * Y, R), F32),
            V((R, WIDTH), BF16), V((R, WIDTH), BF16), V((R, WIDTH), BF16),
            V((16, WIDTH), BF16), V((R + 16, WIDTH), F32),
            V((R, WIDTH), F32), V((R, WIDTH), F32), V((Y, 8, WIDTH), F32), V((Z, 8, WIDTH), F32),
            V((Y, 4 * Y, R), F32), V((Y, WIDTH, R), BF16), V((Y, WIDTH, R), BF16),
            V((WIDTH, R), F32), V((R, 2 * WIDTH), BF16),
            V((X, rows, D), BF16), V((X, rows, D), BF16), V((X, rows, D), F32),
            V((3, rows, D), BF16), V((3, rows, D), BF16),
            dma((8,)), dma((7,)), dma((TP,)), dma((4, H)), dma((2, Z)), dma((Y,)), dma((Y,)),
            dma(()), dma(()), dma((Y,)), dma((Y,)), dma((2, H)), dma((Z,)),
            dma((Y,)), dma((Y,)), dma((Y,)), dma((Y,)), dma(()), dma(()), dma((3,)), dma((3,)),
        ]
        return pl.pallas_call(
            functools.partial(kernel, Z, Y, X),
            out_shape=jax.ShapeDtypeStruct((rows, D), BF16),
            in_specs=[vmem, vmem] + [far] * 6 + [vmem] * 6 + [far] * 2,
            out_specs=vmem,
            scratch_shapes=scratch,
            compiler_params=pltpu.CompilerParams(
                collective_id=0, has_side_effects=True, vmem_limit_bytes=56 * 1024 * 1024
            ),
        )(
            tokens, norm_gain.reshape(1, -1), w_query, w_key, w_value, w_att_gate, w_rec_in,
            w_rec_gate, conv_taps, gate_recur, gate_input, decay_rate.reshape(1, -1),
            head_lambda.reshape(1, 1), head_gain.reshape(1, -1), out_att, out_rec,
        )

    both = P(("sp", "tp"), None)
    cols, lead = P(None, "tp"), P("tp")
    placed = (
        both, P(), cols, cols, cols, cols, cols, cols, cols,
        P("tp", None, None), P("tp", None, None), lead, lead, lead, P("tp", None), P("tp", None),
    )
    return jax.shard_map(body, mesh=mesh, in_specs=placed, out_specs=both, check_vma=False)


def solution(mesh):
    return build(mesh, 4)
```

time: 400 us -> 89.6 us (0.22)
  waiting for transfers between devices: 117 us -> 0 us
  Pallas kernels: 0 us -> 87.2 us
  matrix products: 85.9 us -> 0 us
  local copies, waits for them, and re-layouts: 66.1 us -> 1.57 us
  blocking collectives: 62.6 us -> 0 us
  other arithmetic: 37.4 us -> 0 us
  between operations: 15 us -> 0.66 us
  starting transfers between devices: 11.6 us -> 0 us
    all_gather x1 -> x0, waiting for transfers between devices: 106 us -> none  [side_by_side(): lax.all_gather(both, axis, axis=dim, tiled=True)]
    pallas_call x0 -> x1, Pallas kernels: none -> 87.2 us  [body(): pl.pallas_call(functools.partial(kernel, Z, Y, X), out_shape=jax.ShapeDty...]
    dot_general x69 -> x0, matrix products: 85.9 us -> none  [the longest x32 41.1 us: one_block(): jnp.einsum('phqk,khe->phqe', raised.astype(jnp.bfloat16), value_block, pr...]
    all_gather x2 -> x0, blocking collectives: 35.2 us -> none  [gathered_once(): both, at, found = (lax.all_gather(jnp.concatenate(lines), axis), 0, {})]
    all_to_all x1 -> x0, blocking collectives: 27.4 us -> none  [summed_on_arrival(): blocks = lax.all_to_all(split_up(x, dim, devices), axis, 0, 0, tiled=True)]
    add x126 -> x0, other arithmetic: 21.8 us -> none  [the longest x32 20.7 us: one_block(): key_pos = block_start + jnp.arange(block_len, dtype=jnp.int32)]
    unnamed x32 -> x1, local copies, waits for them, and re-layouts: 23 us -> 1.57 us
    dynamic_slice x32 -> x0, local copies, waits for them, and re-layouts: 18.8 us -> none  [attention(): lax.scan(one_block, running, (key_blocks, value_blocks, block_starts))]
  transfers between devices with their start and end apart: 3 -> 0, of which waited for: 3 -> 0; matrix products, arithmetic and copies ran while one was open for 2% -> 0% of each run, Pallas kernels for 0% -> 0%
where the time goes in v1:
time: 89.6 us; the launch traced here: 89.4 us
  Pallas kernels  87.2 us (97%)
  local copies, waits for them, and re-layouts  1.57 us (2%)
    pallas_call x1, Pallas kernels, body(): pl.pallas_call(functools.partial(kernel, Z, Y, X), out_shape=jax.ShapeDty...  87.2 us

profile of v1, /device:TPU:1, one launch (start us, length us, event | category | flops | bytes accessed | tf_op | source)
XLA Modules:
  0.0 89.4 jit_solution(17574552891824588638)
XLA Ops:
  0.7 87.2 %shard_map.154 = bf16[32,2048]{1,0:T(8,128)(2,1)} custom-call(bf16[32,2048]{1,0:T(8,128)(2,1)} %tokens.1, f32[1,2048]{1,0:T(1,128)} %bitcast.5, bf16[2048,128]{1,0:T(8,128)(2,1)} %w_query.1, bf16[2048,128]{1,0:T(8,128)(2,1)} %w_key.1, bf16[2048,128]{1,0:T(8,128)(2,1)} %w_value.1, bf16[2048,128]{1,0:T(8,128)(2,1)} %w_att_gate.1, bf16[2048,128]{1,0:T(8,128)(2,1)} %w_rec_in.1, ...), custom_call_target="tpu_custom_call" | custom-call | tf_op jit(solution)/shard_map/pallas_call | solution.py:429
  87.8 1.6 %copy.19 = bf16[32,2048]{1,0:T(8,128)(2,1)} copy(bf16[32,2048]{1,0:T(8,128)(2,1)} %shard_map.154) | data formatting | bytes 262144

commit v2 on v1

--- a/solution.py
+++ b/solution.py
@@ -18,6 +18,8 @@
 HEAD_FACTOR = 0.8
 MASKED = -1e30
 LOG2E = math.log2(math.e)
+PIECES = 4
+HALVES = 2
 WIDTH = 128
 
 
@@ -41,6 +43,7 @@
     rows = tokens.shape[0]
     R = xbuf.shape[0]
     H, G = Z // 2, Z - 1 - Z // 2
+    wide = tokens.shape[1] // PIECES
     sp, tp = lax.axis_index("sp"), lax.axis_index("tp")
     z, y = sp // Y, sp % Y
     x, c = tp // 2, tp % 2
@@ -82,28 +85,40 @@
 
     pl.semaphore_wait(barrier, len(peers))
 
-    def ag(slot, device, k):
-        piece = xbuf.at[pl.ds(pl.multiple_of(slot * rows, rows), rows), :]
-        return remote(piece, piece, ag_s.at[k], ag_r.at[slot], device)
+    def ag(slot, device, k, part):
+        piece = xbuf.at[
+            pl.ds(pl.multiple_of(slot * rows, rows), rows), part * wide : (part + 1) * wide
+        ]
+        return remote(piece, piece, ag_s.at[k, part], ag_r.at[slot, part], device)
 
     sent = []
 
     def send(copy):
         copy.start()
         sent.append(copy)
-
-    send(ag(tp, fwd, 0))
-    send(ag(tp, bwd, 1))
-    send(ag(tp, partner, 2))
-    ag(2 * x_bwd + c, fwd, 3).wait_recv()
-    send(ag(2 * x_bwd + c, fwd, 3))
-    send(ag(2 * x_bwd + c, partner, 4))
-    ag(2 * x_fwd + c, partner, 5).wait_recv()
-    send(ag(2 * x_fwd + c, partner, 5))
-    ag(2 * x_far + c, partner, 6).wait_recv()
-    send(ag(2 * x_far + c, partner, 6))
+        return copy
+
+    parts_x = range(PIECES)
+    heads = [send(ag(tp, fwd, 0, q)) for q in parts_x]
+    for q in parts_x:
+        send(ag(tp, partner, 1, q))
+    for copy in heads:
+        copy.wait_send()
+        sent.remove(copy)
+    for q in parts_x:
+        send(ag(tp, bwd, 2, q))
+    for q in parts_x:
+        ag(2 * x_bwd + c, fwd, 3, q).wait_recv()
+        send(ag(2 * x_bwd + c, fwd, 3, q))
+    for q in parts_x:
+        send(ag(2 * x_bwd + c, partner, 4, q))
+    for slot, k in ((2 * x_fwd + c, 5), (2 * x_far + c, 6)):
+        for q in parts_x:
+            ag(slot, partner, k, q).wait_recv()
+            send(ag(slot, partner, k, q))
     for i in range(X):
-        ag(2 * i + 1 - c, partner, 6).wait_recv()
+        for q in parts_x:
+            ag(2 * i + 1 - c, partner, 6, q).wait_recv()
 
     for load in loads[:2]:
         load.wait()
@@ -115,13 +130,15 @@
     bufs = (kbuf, vbuf)
 
     def ring(way_, kind, slot, step):
-        piece = bufs[kind].at[slot]
+        half = bufs[kind // HALVES].shape[1] // HALVES
+        at = kind % HALVES * half
+        piece = bufs[kind // HALVES].at[slot, at : at + half, :]
         return remote(
-            piece, piece, kv_s.at[2 * way_ + kind, step], kv_r.at[kind, slot],
-            (z_up, z_down)[way_],
+            piece, piece, kv_s.at[way_, kind, step], kv_r.at[kind, slot], (z_up, z_down)[way_]
         )
 
-    for kind in range(2):
+    kinds = list(range(2 * HALVES))
+    for kind in kinds:
         ring(0, kind, z, 0).start()
         if G > 0:
             ring(1, kind, z, 0).start()
@@ -141,34 +158,40 @@
     send(remote(rec_s.at[R - 16 :, :], halo, halo_s, halo_r, sp_next))
     recg_s[...] = rr[:, WIDTH:].astype(BF16)
 
-    row = lax.broadcasted_iota(jnp.int32, (R, WIDTH), 0)
-
-    remote(halo, halo, halo_s, halo_r, sp_next).wait_recv()
-    ext[0:16, :] = jnp.where(sp > 0, halo[...].astype(F32), 0.0)
-    ext[16:, :] = rec_s[...].astype(F32)
-    conv = jnp.zeros((R, WIDTH), F32)
-    for j in range(4):
-        conv = conv + ext[13 + j : 13 + j + R, :] * conv_taps[j : j + 1, :]
-    conv_out = conv.astype(BF16)
-    recur = jax.nn.sigmoid(jnp.dot(conv_out, gate_recur[0], preferred_element_type=F32))
-    inflow = jax.nn.sigmoid(jnp.dot(conv_out, gate_input[0], preferred_element_type=F32))
-    log_decay = -RATE_SCALE * recur * decay_rate[...]
-    first = jnp.logical_and(row == 0, sp == 0)
-    factor = jnp.where(first, 1.0, jnp.sqrt(minus_expm1(2.0 * log_decay)))
-    a = jnp.exp(log_decay)
-    b = factor * inflow * conv_out.astype(F32)
-    k = 1
-    while k < R:
-        inside = row >= k
-        b = b + a * jnp.where(inside, pltpu.roll(b, k, 0), 0.0)
-        a = a * jnp.where(inside, pltpu.roll(a, k, 0), 1.0)
-        k *= 2
-    prods[...] = a
-    parts[...] = b
+
     sub = lax.broadcasted_iota(jnp.int32, (8, WIDTH), 0)
-    yagg[y] = jnp.where(sub == 0, a[R - 1 : R, :], b[R - 1 : R, :])
-    for d in range(1, Y):
-        send(remote(yagg.at[y], yagg.at[y], ya_s.at[d], ya_r.at[y], plane(d)))
+
+    def block_scan():
+        row = lax.broadcasted_iota(jnp.int32, (R, WIDTH), 0)
+        remote(halo, halo, halo_s, halo_r, sp_next).wait_recv()
+        ext[0:16, :] = jnp.where(sp > 0, halo[...].astype(F32), 0.0)
+        ext[16:, :] = rec_s[...].astype(F32)
+        conv = jnp.zeros((R, WIDTH), F32)
+        for j in range(4):
+            conv = conv + ext[13 + j : 13 + j + R, :] * conv_taps[j : j + 1, :]
+        conv_out = conv.astype(BF16)
+        recur = jax.nn.sigmoid(jnp.dot(conv_out, gate_recur[0], preferred_element_type=F32))
+        inflow = jax.nn.sigmoid(jnp.dot(conv_out, gate_input[0], preferred_element_type=F32))
+        log_decay = -RATE_SCALE * recur * decay_rate[...]
+        first = jnp.logical_and(row == 0, sp == 0)
+        factor = jnp.where(first, 1.0, jnp.sqrt(minus_expm1(2.0 * log_decay)))
+        a = jnp.exp(log_decay)
+        b = factor * inflow * conv_out.astype(F32)
+        k = 1
+        while k < R:
+            inside = row >= k
+            b = b + a * jnp.where(inside, pltpu.roll(b, k, 0), 0.0)
+            a = a * jnp.where(inside, pltpu.roll(a, k, 0), 1.0)
+            k *= 2
+        prods[...] = a
+        parts[...] = b
+        yagg[y] = jnp.where(sub == 0, a[R - 1 : R, :], b[R - 1 : R, :])
+        for d in range(1, Y):
+            agg_copy(d).start()
+        return
+
+    def agg_copy(d):
+        return remote(yagg.at[y], yagg.at[y], ya_s.at[d], ya_r.at[y], plane(d))
 
     def plane_total():
         for d in range(1, Y):
@@ -207,8 +230,12 @@
         key = kbuf[slot]
         keys = jnp.concatenate([key, key], axis=1)
         value = vbuf[slot]
-        for i in range(2 * Y):
-            s = jnp.dot(keys, qext[i], preferred_element_type=F32)
+        n = 2 * Y
+        score = lambda i: jnp.dot(keys, qext[i], preferred_element_type=F32)
+        scores = [score(i) for i in range(n)]
+
+        for i in range(n):
+            s = scores[i]
             if opening:
                 pos = lax.broadcasted_iota(jnp.int32, (R, R), 1) - lax.broadcasted_iota(
                     jnp.int32, (R, R), 0
@@ -242,9 +269,9 @@
             qext[2 * i + 1] = jnp.concatenate([none, high[half:], none, low[half:]], axis=0)
         tile(z, True)
 
-    def step(s, carry):
+    def pass_on(s, some):
         up, down = (z - s + Z) % Z, (z + s) % Z
-        for kind in range(2):
+        for kind in some:
             ring(0, kind, up, 0).wait_recv()
 
             @pl.when(s < H)
@@ -259,10 +286,27 @@
                 def _():
                     ring(1, kind, down, s).start()
 
+    def step(s, carry):
+        pass_on(s, kinds[:HALVES])
+
         @pl.when(s == 1)
         def _():
+            block_scan()
+
+        @pl.when(jnp.logical_and(s > 1, z >= s - 1))
+        def _():
+            tile((z - s + 1 + Z) % Z, False)
+
+        pass_on(s, kinds[HALVES:])
+
+        @pl.when(s == 1)
+        def _():
             opening()
 
+        @pl.when(jnp.logical_and(s > 1, z + s - 1 >= Z))
+        def _():
+            tile((z + s - 1) % Z, False)
+
         @pl.when(s == 2)
         def _():
             plane_total()
@@ -271,22 +315,20 @@
         def _():
             state_step(s - 2)
 
-        @pl.when(z >= s)
-        def _():
-            tile(up, False)
-
-        @pl.when(jnp.logical_and(s <= G, z + s >= Z))
-        def _():
-            tile(down, False)
-
         return carry
 
     lax.fori_loop(1, H + 1, step, 0)
+
+    @pl.when(z >= H)
+    def _():
+        tile(z - H, False)
 
     stat[y, 0 : 2 * Y, :] = m_ref[0 : 2 * Y, :]
     stat[y, 2 * Y : 4 * Y, :] = l_ref[0 : 2 * Y, :]
     for d in range(1, Y):
         send(remote(stat.at[y], stat.at[y], st_s.at[d], st_r.at[y], plane(d)))
+    if H > 1:
+        state_step(H - 1)
     for d in range(1, Y):
         src = (y + d) % Y
         remote(stat.at[src], stat.at[src], st_s.at[0], st_r.at[src], plane(d)).wait_recv()
@@ -313,11 +355,7 @@
             cbuf[i] = comb.astype(BF16)
             comb_copy(i).start()
 
-    def late(j, carry):
-        state_step(j)
-        return carry
-
-    lax.fori_loop(max(H - 1, 1), H + 1, late, 0)
+    state_step(H)
     h = jnp.zeros((1, WIDTH), F32)
     for i in range(Z - 1):
         h = jnp.where(i < z, zagg[i, 0:1, :] * h + zagg[i, 1:2, :], h)
@@ -346,32 +384,50 @@
             axis=0,
         )
 
-    wo = wout[...]
-    ptx[...] = jnp.dot(group(1 - c), wo, preferred_element_type=F32).astype(BF16).reshape(ptx.shape)
-    send(remote(ptx, prx, pr_s, pr_r, partner))
-    own_o[...] = jnp.dot(group(c), wo, preferred_element_type=F32).reshape(own_o.shape)
-    remote(ptx, prx, pr_s, pr_r, partner).wait_recv()
-
-    def both(i):
-        return own_o[i] + prx[i].astype(F32)
-
-    def hop(k, device):
-        return remote(rtx.at[k], rrx.at[k], rs_s.at[k], rs_r.at[k], device)
-
-    rtx[0] = both(x_far).astype(BF16)
-    send(hop(0, fwd))
-    rtx[1] = both(x_bwd).astype(BF16)
-    send(hop(1, bwd))
-    hop(0, fwd).wait_recv()
-    rtx[2] = (both(x_fwd) + rrx[0].astype(F32)).astype(BF16)
-    send(hop(2, fwd))
-    hop(1, bwd).wait_recv()
-    mine = both(x) + rrx[1].astype(F32)
-    hop(2, fwd).wait_recv()
-    out[...] = (mine + rrx[2].astype(F32)).astype(BF16)
+    def cols(q):
+        return slice(q * wide, (q + 1) * wide)
+
+    def swap(q):
+        return remote(ptx.at[:, :, cols(q)], prx.at[:, :, cols(q)], pr_s.at[q], pr_r.at[q], partner)
+
+    theirs, ours = group(1 - c), group(c)
+    for q in parts_x:
+        part = jnp.dot(theirs, wout[:, cols(q)], preferred_element_type=F32)
+        ptx[:, :, cols(q)] = part.astype(BF16).reshape(X, rows, wide)
+        send(swap(q))
+    for q in parts_x:
+        part = jnp.dot(ours, wout[:, cols(q)], preferred_element_type=F32)
+        own_o[:, :, cols(q)] = part.reshape(X, rows, wide)
+
+    def both(i, q):
+        return own_o[i, :, cols(q)] + prx[i, :, cols(q)].astype(F32)
+
+    def hop(k, q, device):
+        return remote(
+            rtx.at[k, :, cols(q)], rrx.at[k, :, cols(q)], rs_s.at[k, q], rs_r.at[k, q], device
+        )
+
+    for q in parts_x:
+        swap(q).wait_recv()
+        rtx[0, :, cols(q)] = both(x_far, q).astype(BF16)
+        send(hop(0, q, fwd))
+    for q in parts_x:
+        rtx[1, :, cols(q)] = both(x_bwd, q).astype(BF16)
+        send(hop(1, q, bwd))
+    for q in parts_x:
+        hop(0, q, fwd).wait_recv()
+        rtx[2, :, cols(q)] = (both(x_fwd, q) + rrx[0, :, cols(q)].astype(F32)).astype(BF16)
+        send(hop(2, q, fwd))
+    for q in parts_x:
+        hop(1, q, bwd).wait_recv()
+        mine = both(x, q) + rrx[1, :, cols(q)].astype(F32)
+        hop(2, q, fwd).wait_recv()
+        out[:, cols(q)] = (mine + rrx[2, :, cols(q)].astype(F32)).astype(BF16)
 
     for copy in sent:
         copy.wait_send()
+    for d in range(1, Y):
+        agg_copy(d).wait_send()
     for i in range(Y):
 
         @pl.when(y != i)
@@ -379,7 +435,7 @@
             comb_copy(i).wait_send()
 
     def drain(s, carry):
-        for kind in range(2):
+        for kind in kinds:
             ring(0, kind, z, s).wait_send()
 
             @pl.when(s < G)
@@ -422,9 +478,9 @@
             V((WIDTH, R), F32), V((R, 2 * WIDTH), BF16),
             V((X, rows, D), BF16), V((X, rows, D), BF16), V((X, rows, D), F32),
             V((3, rows, D), BF16), V((3, rows, D), BF16),
-            dma((8,)), dma((7,)), dma((TP,)), dma((4, H)), dma((2, Z)), dma((Y,)), dma((Y,)),
+            dma((8,)), dma((7, PIECES)), dma((TP, PIECES)), dma((2, 2 * HALVES, H)), dma((2 * HALVES, Z)), dma((Y,)), dma((Y,)),
             dma(()), dma(()), dma((Y,)), dma((Y,)), dma((2, H)), dma((Z,)),
-            dma((Y,)), dma((Y,)), dma((Y,)), dma((Y,)), dma(()), dma(()), dma((3,)), dma((3,)),
+            dma((Y,)), dma((Y,)), dma((Y,)), dma((Y,)), dma((PIECES,)), dma((PIECES,)), dma((3, PIECES)), dma((3, PIECES)),
         ]
         return pl.pallas_call(
             functools.partial(kernel, Z, Y, X),

time: 89.6 us -> 78.6 us (0.88)
  Pallas kernels: 87.2 us -> 76.2 us
    pallas_call x1, Pallas kernels: 87.2 us -> 76.2 us  [body(): pl.pallas_call(functools.partial(kernel, Z, Y, X), out_shape=jax.ShapeDty...]
where the time goes in v2:
time: 78.6 us; the launch traced here: 78.4 us
  Pallas kernels  76.2 us (97%)
  local copies, waits for them, and re-layouts  1.57 us (2%)
    pallas_call x1, Pallas kernels, body(): pl.pallas_call(functools.partial(kernel, Z, Y, X), out_shape=jax.ShapeDty...  76.2 us

profile of v2, /device:TPU:1, one launch (start us, length us, event | category | flops | bytes accessed | tf_op | source)
XLA Modules:
  0.0 78.4 jit_solution(11889203538106343251)
XLA Ops:
  0.7 76.2 %shard_map.154 = bf16[32,2048]{1,0:T(8,128)(2,1)} custom-call(bf16[32,2048]{1,0:T(8,128)(2,1)} %tokens.1, f32[1,2048]{1,0:T(1,128)} %bitcast.5, bf16[2048,128]{1,0:T(8,128)(2,1)} %w_query.1, bf16[2048,128]{1,0:T(8,128)(2,1)} %w_key.1, bf16[2048,128]{1,0:T(8,128)(2,1)} %w_value.1, bf16[2048,128]{1,0:T(8,128)(2,1)} %w_att_gate.1, bf16[2048,128]{1,0:T(8,128)(2,1)} %w_rec_in.1, ...), custom_call_target="tpu_custom_call" | custom-call | tf_op jit(solution)/shard_map/pallas_call | solution.py:485
  76.8 1.6 %copy.19 = bf16[32,2048]{1,0:T(8,128)(2,1)} copy(bf16[32,2048]{1,0:T(8,128)(2,1)} %shard_map.154) | data formatting | bytes 262144

commit v3 on v2

--- a/solution.py
+++ b/solution.py
@@ -35,10 +35,10 @@
     tokens, norm_gain, w_query, w_key, w_value, w_att_gate, w_rec_in, w_rec_gate, conv_taps,
     gate_recur, gate_input, decay_rate, head_lambda, head_gain, out_att, out_rec,
     out,
-    wcat, wout, xbuf, kbuf, vbuf, qbuf, qext, acc, m_ref, l_ref, gate_s, rec_s, recg_s, halo, ext,
-    prods, parts, yagg, zagg, stat, cbuf, pbuf, own_c, mixed, ptx, prx, own_o, rtx, rrx,
-    w_sem, ag_s, ag_r, kv_s, kv_r, q_s, q_r, halo_s, halo_r, ya_s, ya_r, za_s, za_r,
-    st_s, st_r, cb_s, cb_r, pr_s, pr_r, rs_s, rs_r,
+    wcat, wfull, xbuf, kbuf, vbuf, qbuf, qext, acc, m_ref, l_ref, last_p, last_f, gate_s, rec_s, recg_s, halo, ext,
+    prods, parts, yagg, zagg, stat, cbuf, pbuf, own_c, att_m, rec_m, att_g, rec_g, out_a,
+    w_sem, ag_s, ag_r, ag_p, kv_s, kv_r, q_s, q_r, halo_s, halo_r, ya_s, ya_r, za_s, za_r,
+    st_s, st_r, cb_s, cb_r, wg_s, wg_r, wg_p, am_s, am_r, rm_s, rm_r,
 ):
     rows = tokens.shape[0]
     R = xbuf.shape[0]
@@ -57,25 +57,37 @@
     def plane(d):
         return (z * Y + (y + d) % Y, tp)
 
+    def row_peer(d):
+        return (sp, (tp + d) % (2 * X))
+
     def remote(src, dst, send, recv, device):
         return pltpu.make_async_remote_copy(
             src_ref=src, dst_ref=dst, send_sem=send, recv_sem=recv,
             device_id=device, device_id_type=MESH,
         )
 
+    def all_sent(piece, sem):
+        remote(piece, piece, sem, sem, partner).wait_send()
+
+    def all_here(piece, sem):
+        remote(piece, piece, sem, sem, partner).wait_recv()
+
     loads = [
         pltpu.make_async_copy(w, wcat.at[:, i * WIDTH : (i + 1) * WIDTH], w_sem.at[i])
         for i, w in enumerate((w_key, w_value, w_query, w_att_gate, w_rec_in, w_rec_gate))
     ]
     loads += [
-        pltpu.make_async_copy(w, wout.at[i * WIDTH : (i + 1) * WIDTH, :], w_sem.at[6 + i])
-        for i, w in enumerate((out_att, out_rec))
+        pltpu.make_async_copy(
+            w, wfull.at[i, pl.ds(pl.multiple_of(tp * WIDTH, WIDTH), WIDTH), :], w_sem.at[6 + i]
+        )
+        for i, w in enumerate((out_rec, out_att))
     ]
     for load in loads:
         load.start()
 
     barrier = pltpu.get_barrier_semaphore()
-    peers = [partner, fwd, bwd, z_up, z_down, sp_next, sp_prev] + [plane(d) for d in range(1, Y)]
+    peers = [z_up, z_down, sp_next, sp_prev] + [plane(d) for d in range(1, Y)]
+    peers += [row_peer(d) for d in range(1, 2 * X)]
     for peer in peers:
         pl.semaphore_signal(barrier, inc=1, device_id=peer, device_id_type=MESH)
 
@@ -85,40 +97,80 @@
 
     pl.semaphore_wait(barrier, len(peers))
 
-    def ag(slot, device, k, part):
+    def block(slot):
+        return xbuf.at[pl.ds(pl.multiple_of(slot * rows, rows), rows), :]
+
+    def ag(slot, device, k, part, recv):
         piece = xbuf.at[
             pl.ds(pl.multiple_of(slot * rows, rows), rows), part * wide : (part + 1) * wide
         ]
-        return remote(piece, piece, ag_s.at[k, part], ag_r.at[slot, part], device)
-
-    sent = []
-
-    def send(copy):
-        copy.start()
-        sent.append(copy)
-        return copy
+        return remote(piece, piece, ag_s.at[k], recv, device)
+
+    def ag_near(slot, device, k, part):
+        return ag(slot, device, k, part, ag_r.at[slot // 2, part])
+
+    def ag_over(slot, k, part):
+        return ag(slot, partner, k, part, ag_p.at[slot // 2])
 
     parts_x = range(PIECES)
-    heads = [send(ag(tp, fwd, 0, q)) for q in parts_x]
-    for q in parts_x:
-        send(ag(tp, partner, 1, q))
-    for copy in heads:
-        copy.wait_send()
-        sent.remove(copy)
-    for q in parts_x:
-        send(ag(tp, bwd, 2, q))
-    for q in parts_x:
-        ag(2 * x_bwd + c, fwd, 3, q).wait_recv()
-        send(ag(2 * x_bwd + c, fwd, 3, q))
-    for q in parts_x:
-        send(ag(2 * x_bwd + c, partner, 4, q))
+    for q in parts_x:
+        ag_near(tp, fwd, 0, q).start()
+    for q in parts_x:
+        ag_over(tp, 1, q).start()
+    all_sent(block(tp), ag_s.at[0])
+    for q in parts_x:
+        ag_near(tp, bwd, 2, q).start()
+    for q in parts_x:
+        ag_near(2 * x_bwd + c, fwd, 3, q).wait_recv()
+        ag_near(2 * x_bwd + c, fwd, 3, q).start()
+    for q in parts_x:
+        ag_over(2 * x_bwd + c, 4, q).start()
     for slot, k in ((2 * x_fwd + c, 5), (2 * x_far + c, 6)):
         for q in parts_x:
-            ag(slot, partner, k, q).wait_recv()
-            send(ag(slot, partner, k, q))
+            ag_near(slot, fwd, k, q).wait_recv()
+            ag_over(slot, k, q).start()
     for i in range(X):
-        for q in parts_x:
-            ag(2 * i + 1 - c, partner, 6, q).wait_recv()
+        all_here(block(2 * i + 1 - c), ag_p.at[i])
+
+    per = max(H // 2, 1)
+    tall = WIDTH // per
+
+    def weights(slot, device, k, q):
+        at = pl.multiple_of(slot * WIDTH + q % per * tall, tall)
+        piece = wfull.at[q // per, pl.ds(at, tall), :]
+        recv = wg_r.at[slot // 2, q] if k in (0, 1, 3) else wg_p.at[q // per, slot // 2]
+        return remote(piece, piece, wg_s.at[k], recv, device)
+
+    def own_weights(q):
+        weights(tp, fwd, 0, q).start()
+        weights(tp, bwd, 1, q).start()
+        weights(tp, partner, 2, q).start()
+
+    def weights_step(s):
+        @pl.when(jnp.logical_and(s >= 2, s - 2 < H))
+        def _():
+            q = s - 2
+            turn = way * (1 - 2 * (q % 2))
+            src, dst = (x - turn + X) % X, (x + turn + X) % X
+            weights(2 * src + c, fwd, 3, q).wait_recv()
+            weights(2 * src + c, (sp, 2 * dst + c), 3, q).start()
+            weights(2 * src + c, partner, 4, q).start()
+            weights(2 * dst + c, fwd, 3, q).wait_recv()
+            weights(2 * dst + c, partner, 5, q).start()
+
+        @pl.when(s + 1 < H)
+        def _():
+            own_weights(s + 1)
+
+        @pl.when(jnp.logical_and(s >= 4, s - 4 < H))
+        def _():
+            weights(2 * x_far + c, fwd, 3, s - 4).wait_recv()
+            weights(2 * x_far + c, partner, 6, s - 4).start()
+
+    def weights_here(kind):
+        for i in range(X):
+            at = pl.multiple_of((2 * i + 1 - c) * WIDTH, WIDTH)
+            all_here(wfull.at[kind, pl.ds(at, WIDTH), :], wg_p.at[kind, i])
 
     for load in loads[:2]:
         load.wait()
@@ -134,7 +186,7 @@
         at = kind % HALVES * half
         piece = bufs[kind // HALVES].at[slot, at : at + half, :]
         return remote(
-            piece, piece, kv_s.at[way_, kind, step], kv_r.at[kind, slot], (z_up, z_down)[way_]
+            piece, piece, kv_s.at[way_, kind // HALVES], kv_r.at[kind, slot], (z_up, z_down)[way_]
         )
 
     kinds = list(range(2 * HALVES))
@@ -148,14 +200,16 @@
     qg = jnp.dot(normed, wcat[:, 2 * WIDTH : 4 * WIDTH], preferred_element_type=F32)
     qbuf[y] = qg[:, :WIDTH].T.astype(BF16)
     for d in range(1, Y):
-        send(remote(qbuf.at[y], qbuf.at[y], q_s.at[d], q_r.at[y], plane(d)))
+        remote(qbuf.at[y], qbuf.at[y], q_s, q_r, plane(d)).start()
     gate_s[...] = qg[:, WIDTH:].astype(BF16)
 
     for load in loads[4:]:
         load.wait()
+    for q in range(min(2, H)):
+        own_weights(q)
     rr = jnp.dot(normed, wcat[:, 4 * WIDTH :], preferred_element_type=F32)
     rec_s[...] = rr[:, :WIDTH].astype(BF16)
-    send(remote(rec_s.at[R - 16 :, :], halo, halo_s, halo_r, sp_next))
+    remote(rec_s.at[R - 16 :, :], halo, halo_s, halo_r, sp_next).start()
     recg_s[...] = rr[:, WIDTH:].astype(BF16)
 
 
@@ -191,12 +245,10 @@
         return
 
     def agg_copy(d):
-        return remote(yagg.at[y], yagg.at[y], ya_s.at[d], ya_r.at[y], plane(d))
+        return remote(yagg.at[y], yagg.at[y], ya_s, ya_r, plane(d))
 
     def plane_total():
-        for d in range(1, Y):
-            src = (y + d) % Y
-            remote(yagg.at[src], yagg.at[src], ya_s.at[0], ya_r.at[src], plane(d)).wait_recv()
+        all_here(yagg.at[0 : Y - 1], ya_r)
         ta, tb = yagg[0, 0:1, :], yagg[0, 1:2, :]
         for i in range(1, Y):
             ia, ib = yagg[i, 0:1, :], yagg[i, 1:2, :]
@@ -208,7 +260,7 @@
 
     def state(way_, slot, step):
         piece = zagg.at[slot]
-        return remote(piece, piece, za_s.at[way_, step], za_r.at[slot], (z_up, z_down)[way_])
+        return remote(piece, piece, za_s.at[way_], za_r.at[slot], (z_up, z_down)[way_])
 
     def state_step(j):
         up, down = (z - j + Z) % Z, (z + j) % Z
@@ -255,10 +307,29 @@
                 acc[i] = acc[i] * fade + jnp.dot(value, p.astype(BF16), preferred_element_type=F32)
             m_ref[i : i + 1, :] = top
 
+    def last_scores(slot):
+        key = kbuf[slot]
+        keys = jnp.concatenate([key, key], axis=1)
+        scores = [jnp.dot(keys, qext[i], preferred_element_type=F32) for i in range(2 * Y)]
+        for i in range(2 * Y):
+            old = m_ref[i : i + 1, :]
+            top = jnp.maximum(old, jnp.max(scores[i], axis=0, keepdims=True))
+            p = jnp.exp2(scores[i] - top)
+            fade = jnp.exp2(old - top)
+            l_ref[i : i + 1, :] = l_ref[i : i + 1, :] * fade + jnp.sum(p, axis=0, keepdims=True)
+            last_p[i] = p.astype(BF16)
+            last_f[i : i + 1, :] = fade
+            m_ref[i : i + 1, :] = top
+
+    def last_values(slot):
+        value = vbuf[slot]
+        for i in range(2 * Y):
+            acc[i] = acc[i] * last_f[i : i + 1, :] + jnp.dot(
+                value, last_p[i], preferred_element_type=F32
+            )
+
     def opening():
-        for d in range(1, Y):
-            src = (y + d) % Y
-            remote(qbuf.at[src], qbuf.at[src], q_s.at[0], q_r.at[src], plane(d)).wait_recv()
+        all_here(qbuf.at[0 : Y - 1], q_r)
         half = WIDTH // 2
         none = jnp.zeros((half, R), BF16)
         for i in range(Y):
@@ -297,7 +368,9 @@
         def _():
             tile((z - s + 1 + Z) % Z, False)
 
-        pass_on(s, kinds[HALVES:])
+        @pl.when(s < H)
+        def _():
+            pass_on(s, kinds[HALVES:])
 
         @pl.when(s == 1)
         def _():
@@ -315,27 +388,30 @@
         def _():
             state_step(s - 2)
 
+        weights_step(s)
         return carry
 
     lax.fori_loop(1, H + 1, step, 0)
 
     @pl.when(z >= H)
     def _():
-        tile(z - H, False)
+        last_scores(z - H)
 
     stat[y, 0 : 2 * Y, :] = m_ref[0 : 2 * Y, :]
     stat[y, 2 * Y : 4 * Y, :] = l_ref[0 : 2 * Y, :]
     for d in range(1, Y):
-        send(remote(stat.at[y], stat.at[y], st_s.at[d], st_r.at[y], plane(d)))
-    if H > 1:
-        state_step(H - 1)
-    for d in range(1, Y):
-        src = (y + d) % Y
-        remote(stat.at[src], stat.at[src], st_s.at[0], st_r.at[src], plane(d)).wait_recv()
+        remote(stat.at[y], stat.at[y], st_s, st_r, plane(d)).start()
+    pass_on(jnp.int32(H), kinds[HALVES:])
+
+    @pl.when(z >= H)
+    def _():
+        last_values(z - H)
+
+    all_here(stat.at[0 : Y - 1], st_r)
     lam = head_lambda[...]
 
     def comb_copy(i):
-        return remote(cbuf.at[i], pbuf.at[y], cb_s.at[i], cb_r.at[y], (z * Y + i, tp))
+        return remote(cbuf.at[i], pbuf.at[y], cb_s, cb_r, (z * Y + i, tp))
 
     for i in range(Y):
         weight = []
@@ -355,7 +431,11 @@
             cbuf[i] = comb.astype(BF16)
             comb_copy(i).start()
 
+    weights_step(jnp.int32(H + 1))
+    if H > 1:
+        state_step(H - 1)
     state_step(H)
+
     h = jnp.zeros((1, WIDTH), F32)
     for i in range(Z - 1):
         h = jnp.where(i < z, zagg[i, 0:1, :] * h + zagg[i, 1:2, :], h)
@@ -363,94 +443,65 @@
         h = jnp.where(i < y, yagg[i, 0:1, :] * h + yagg[i, 1:2, :], h)
     states = parts[...] + prods[...] * h
     recg = recg_s[...].astype(F32)
-    mixed[:, WIDTH:] = (states * (recg * jax.nn.sigmoid(recg))).astype(BF16)
-
+    rec_m[...] = (states * (recg * jax.nn.sigmoid(recg))).astype(BF16)
+
+    def share(mine, theirs, ss, rs, d):
+        peer = (tp + d) % (2 * X)
+        piece = mine.at[pl.ds(pl.multiple_of(peer * rows, rows), rows), :]
+        return remote(piece, theirs.at[tp], ss, rs, row_peer(d))
+
+    def shared(mine, theirs, ss, rs):
+        all_here(theirs.at[0 : 2 * X - 1], rs)
+        theirs[tp] = mine[pl.ds(pl.multiple_of(tp * rows, rows), rows), :]
+        return jnp.concatenate([theirs[i] for i in range(2 * X)], axis=1)
+
+    for way_, count in ((0, H), (1, G)):
+        if count > 0:
+            all_sent(kbuf.at[0:count], kv_s.at[way_, 0])
+            all_sent(vbuf.at[0:count], kv_s.at[way_, 1])
+            all_sent(zagg.at[0:count], za_s.at[way_])
+    if Y > 1:
+        all_sent(yagg.at[0 : Y - 1], ya_s)
+        all_sent(qbuf.at[0 : Y - 1], q_s)
+        all_sent(stat.at[0 : Y - 1], st_s)
+    all_sent(halo, halo_s)
+    weights_step(jnp.int32(H + 2))
+    for d in range(1, 2 * X):
+        share(rec_m, rec_g, rm_s, rm_r, d).start()
     total = own_c[...]
+    all_here(pbuf.at[0 : Y - 1], cb_r)
     for d in range(1, Y):
-        src = (y + d) % Y
-        remote(pbuf.at[src], pbuf.at[src], cb_s.at[0], cb_r.at[src], plane(d)).wait_recv()
-        total = total + pbuf[src].astype(F32)
+        total = total + pbuf[(y + d) % Y].astype(F32)
     total = total * lax.rsqrt(jnp.mean(total * total, axis=0, keepdims=True) + EPS_HEAD)
     gate = gate_s[...].astype(F32)
     att = total.T * head_gain[...] * HEAD_FACTOR * (gate * jax.nn.sigmoid(gate))
-    mixed[:, :WIDTH] = att.astype(BF16)
-
-    def group(core):
-        return jnp.concatenate(
-            [
-                mixed[pl.ds(pl.multiple_of((2 * i + core) * rows, rows), rows), :]
-                for i in range(X)
-            ],
-            axis=0,
-        )
-
-    def cols(q):
-        return slice(q * wide, (q + 1) * wide)
-
-    def swap(q):
-        return remote(ptx.at[:, :, cols(q)], prx.at[:, :, cols(q)], pr_s.at[q], pr_r.at[q], partner)
-
-    theirs, ours = group(1 - c), group(c)
-    for q in parts_x:
-        part = jnp.dot(theirs, wout[:, cols(q)], preferred_element_type=F32)
-        ptx[:, :, cols(q)] = part.astype(BF16).reshape(X, rows, wide)
-        send(swap(q))
-    for q in parts_x:
-        part = jnp.dot(ours, wout[:, cols(q)], preferred_element_type=F32)
-        own_o[:, :, cols(q)] = part.reshape(X, rows, wide)
-
-    def both(i, q):
-        return own_o[i, :, cols(q)] + prx[i, :, cols(q)].astype(F32)
-
-    def hop(k, q, device):
-        return remote(
-            rtx.at[k, :, cols(q)], rrx.at[k, :, cols(q)], rs_s.at[k, q], rs_r.at[k, q], device
-        )
-
-    for q in parts_x:
-        swap(q).wait_recv()
-        rtx[0, :, cols(q)] = both(x_far, q).astype(BF16)
-        send(hop(0, q, fwd))
-    for q in parts_x:
-        rtx[1, :, cols(q)] = both(x_bwd, q).astype(BF16)
-        send(hop(1, q, bwd))
-    for q in parts_x:
-        hop(0, q, fwd).wait_recv()
-        rtx[2, :, cols(q)] = (both(x_fwd, q) + rrx[0, :, cols(q)].astype(F32)).astype(BF16)
-        send(hop(2, q, fwd))
-    for q in parts_x:
-        hop(1, q, bwd).wait_recv()
-        mine = both(x, q) + rrx[1, :, cols(q)].astype(F32)
-        hop(2, q, fwd).wait_recv()
-        out[:, cols(q)] = (mine + rrx[2, :, cols(q)].astype(F32)).astype(BF16)
-
-    for copy in sent:
-        copy.wait_send()
-    for d in range(1, Y):
-        agg_copy(d).wait_send()
-    for i in range(Y):
-
-        @pl.when(y != i)
-        def _():
-            comb_copy(i).wait_send()
-
-    def drain(s, carry):
-        for kind in kinds:
-            ring(0, kind, z, s).wait_send()
-
-            @pl.when(s < G)
-            def _():
-                ring(1, kind, z, s).wait_send()
-
-        state(0, z, s).wait_send()
-
-        @pl.when(s < G)
-        def _():
-            state(1, z, s).wait_send()
-
-        return carry
-
-    lax.fori_loop(0, H, drain, 0)
+    att_m[...] = att.astype(BF16)
+    for d in range(1, 2 * X):
+        share(att_m, att_g, am_s, am_r, d).start()
+
+    weights_step(jnp.int32(H + 3))
+
+    mine = pl.ds(pl.multiple_of(tp * WIDTH, WIDTH), WIDTH)
+    for k in range(7):
+        all_sent(wfull.at[:, mine, :], wg_s.at[k])
+    for k in range(1, 7):
+        all_sent(block(tp), ag_s.at[k])
+    all_sent(pbuf.at[0 : Y - 1], cb_s)
+    all_sent(rec_m.at[0 : (2 * X - 1) * rows, :], rm_s)
+    weights_here(0)
+    left = shared(rec_m, rec_g, rm_s, rm_r)
+    for q in parts_x:
+        cols = slice(q * wide, (q + 1) * wide)
+        out_a[:, cols] = jnp.dot(left, wfull[0, :, cols], preferred_element_type=F32)
+    if H > 1:
+        weights_here(1)
+    left = shared(att_m, att_g, am_s, am_r)
+    for q in parts_x:
+        cols = slice(q * wide, (q + 1) * wide)
+        part = jnp.dot(left, wfull[1, :, cols], preferred_element_type=F32)
+        out[:, cols] = (out_a[:, cols] + part).astype(BF16)
+
+    all_sent(att_m.at[0 : (2 * X - 1) * rows, :], am_s)
 
 
 def build(mesh, Y):
@@ -467,20 +518,20 @@
         vmem, far = pl.BlockSpec(memory_space=pltpu.VMEM), pl.BlockSpec(memory_space=pl.ANY)
         V, dma = pltpu.VMEM, pltpu.SemaphoreType.DMA
         scratch = [
-            V((D, 6 * WIDTH), BF16), V((2 * WIDTH, D), BF16), V((R, D), BF16),
+            V((D, 6 * WIDTH), BF16), V((2, TP * WIDTH, D), BF16), V((R, D), BF16),
             V((Z, R, WIDTH), BF16), V((Z, WIDTH, R), BF16), V((Y, WIDTH, R), BF16),
             V((2 * Y, 2 * WIDTH, R), BF16), V((2 * Y, WIDTH, R), F32),
-            V((2 * Y, R), F32), V((2 * Y, R), F32),
+            V((2 * Y, R), F32), V((2 * Y, R), F32), V((2 * Y, R, R), BF16), V((2 * Y, R), F32),
             V((R, WIDTH), BF16), V((R, WIDTH), BF16), V((R, WIDTH), BF16),
             V((16, WIDTH), BF16), V((R + 16, WIDTH), F32),
             V((R, WIDTH), F32), V((R, WIDTH), F32), V((Y, 8, WIDTH), F32), V((Z, 8, WIDTH), F32),
             V((Y, 4 * Y, R), F32), V((Y, WIDTH, R), BF16), V((Y, WIDTH, R), BF16),
-            V((WIDTH, R), F32), V((R, 2 * WIDTH), BF16),
-            V((X, rows, D), BF16), V((X, rows, D), BF16), V((X, rows, D), F32),
-            V((3, rows, D), BF16), V((3, rows, D), BF16),
-            dma((8,)), dma((7, PIECES)), dma((TP, PIECES)), dma((2, 2 * HALVES, H)), dma((2 * HALVES, Z)), dma((Y,)), dma((Y,)),
-            dma(()), dma(()), dma((Y,)), dma((Y,)), dma((2, H)), dma((Z,)),
-            dma((Y,)), dma((Y,)), dma((Y,)), dma((Y,)), dma((PIECES,)), dma((PIECES,)), dma((3, PIECES)), dma((3, PIECES)),
+            V((WIDTH, R), F32), V((R, WIDTH), BF16), V((R, WIDTH), BF16),
+            V((TP, rows, WIDTH), BF16), V((TP, rows, WIDTH), BF16), V((rows, D), F32),
+            dma((8,)), dma((7,)), dma((X, PIECES)), dma((X,)), dma((2, 2)), dma((2 * HALVES, Z)),
+            dma(()), dma(()), dma(()), dma(()), dma(()), dma(()), dma((2,)), dma((Z,)),
+            dma(()), dma(()), dma(()), dma(()), dma((7,)), dma((X, H)), dma((2, X)),
+            dma(()), dma(()), dma(()), dma(()),
         ]
         return pl.pallas_call(
             functools.partial(kernel, Z, Y, X),

time: 78.6 us -> 75.4 us (0.959)
  Pallas kernels: 76.2 us -> 73.1 us
    pallas_call x1, Pallas kernels: 76.2 us -> 73.1 us  [body(): pl.pallas_call(functools.partial(kernel, Z, Y, X), out_shape=jax.ShapeDty...]
where the time goes in v3:
time: 75.4 us; the launch traced here: 75.3 us
  Pallas kernels  73.1 us (97%)
  local copies, waits for them, and re-layouts  1.57 us (2%)
    pallas_call x1, Pallas kernels, body(): pl.pallas_call(functools.partial(kernel, Z, Y, X), out_shape=jax.ShapeDty...  73.1 us
    unnamed x1, local copies, waits for them, and re-layouts  1.57 us

profile of v3, /device:TPU:1, one launch (start us, length us, event | category | flops | bytes accessed | tf_op | source)
XLA Modules:
  0.0 75.3 jit_solution(5383406298918899852)
XLA Ops:
  0.7 73.1 %shard_map.154 = bf16[32,2048]{1,0:T(8,128)(2,1)} custom-call(bf16[32,2048]{1,0:T(8,128)(2,1)} %tokens.1, f32[1,2048]{1,0:T(1,128)} %bitcast.5, bf16[2048,128]{1,0:T(8,128)(2,1)} %w_query.1, bf16[2048,128]{1,0:T(8,128)(2,1)} %w_key.1, bf16[2048,128]{1,0:T(8,128)(2,1)} %w_value.1, bf16[2048,128]{1,0:T(8,128)(2,1)} %w_att_gate.1, bf16[2048,128]{1,0:T(8,128)(2,1)} %w_rec_in.1, ...), custom_call_target="tpu_custom_call" | custom-call | tf_op jit(solution)/shard_map/pallas_call | solution.py:536
  73.7 1.6 %copy.19 = bf16[32,2048]{1,0:T(8,128)(2,1)} copy(bf16[32,2048]{1,0:T(8,128)(2,1)} %shard_map.154) | data formatting | bytes 262144

commit v4 on v3

--- a/solution.py
+++ b/solution.py
@@ -407,6 +407,9 @@
     def _():
         last_values(z - H)
 
+    weights_step(jnp.int32(H + 1))
+    if H > 1:
+        state_step(H - 1)
     all_here(stat.at[0 : Y - 1], st_r)
     lam = head_lambda[...]
 
@@ -426,14 +429,11 @@
         def _():
             own_c[...] = comb
 
-        @pl.when(y != i)
-        def _():
-            cbuf[i] = comb.astype(BF16)
-            comb_copy(i).start()
-
-    weights_step(jnp.int32(H + 1))
-    if H > 1:
-        state_step(H - 1)
+        cbuf[i] = comb.astype(BF16)
+
+    for d in sorted(range(1, Y), key=lambda d: -min(d, Y - d)):
+        comb_copy((y + d) % Y).start()
+
     state_step(H)
 
     h = jnp.zeros((1, WIDTH), F32)
@@ -455,6 +455,8 @@
         theirs[tp] = mine[pl.ds(pl.multiple_of(tp * rows, rows), rows), :]
         return jnp.concatenate([theirs[i] for i in range(2 * X)], axis=1)
 
+    for d in range(1, 2 * X):
+        share(rec_m, rec_g, rm_s, rm_r, d).start()
     for way_, count in ((0, H), (1, G)):
         if count > 0:
             all_sent(kbuf.at[0:count], kv_s.at[way_, 0])
@@ -466,8 +468,6 @@
         all_sent(stat.at[0 : Y - 1], st_s)
     all_sent(halo, halo_s)
     weights_step(jnp.int32(H + 2))
-    for d in range(1, 2 * X):
-        share(rec_m, rec_g, rm_s, rm_r, d).start()
     total = own_c[...]
     all_here(pbuf.at[0 : Y - 1], cb_r)
     for d in range(1, Y):
@@ -481,6 +481,19 @@
 
     weights_step(jnp.int32(H + 3))
 
+    weights_here(0)
+    left = shared(rec_m, rec_g, rm_s, rm_r)
+    for q in parts_x:
+        cols = slice(q * wide, (q + 1) * wide)
+        out_a[:, cols] = jnp.dot(left, wfull[0, :, cols], preferred_element_type=F32)
+    if H > 1:
+        weights_here(1)
+    left = shared(att_m, att_g, am_s, am_r)
+    for q in parts_x:
+        cols = slice(q * wide, (q + 1) * wide)
+        part = jnp.dot(left, wfull[1, :, cols], preferred_element_type=F32)
+        out[:, cols] = (out_a[:, cols] + part).astype(BF16)
+
     mine = pl.ds(pl.multiple_of(tp * WIDTH, WIDTH), WIDTH)
     for k in range(7):
         all_sent(wfull.at[:, mine, :], wg_s.at[k])
@@ -488,19 +501,6 @@
         all_sent(block(tp), ag_s.at[k])
     all_sent(pbuf.at[0 : Y - 1], cb_s)
     all_sent(rec_m.at[0 : (2 * X - 1) * rows, :], rm_s)
-    weights_here(0)
-    left = shared(rec_m, rec_g, rm_s, rm_r)
-    for q in parts_x:
-        cols = slice(q * wide, (q + 1) * wide)
-        out_a[:, cols] = jnp.dot(left, wfull[0, :, cols], preferred_element_type=F32)
-    if H > 1:
-        weights_here(1)
-    left = shared(att_m, att_g, am_s, am_r)
-    for q in parts_x:
-        cols = slice(q * wide, (q + 1) * wide)
-        part = jnp.dot(left, wfull[1, :, cols], preferred_element_type=F32)
-        out[:, cols] = (out_a[:, cols] + part).astype(BF16)
-
     all_sent(att_m.at[0 : (2 * X - 1) * rows, :], am_s)
 
 

time: 75.4 us -> 75 us (level)
  no operation moved by 1% of the time
where the time goes in v4:
time: 75 us; the launch traced here: 74.9 us
  Pallas kernels  72.7 us (97%)
  local copies, waits for them, and re-layouts  1.57 us (2%)
    pallas_call x1, Pallas kernels, body(): pl.pallas_call(functools.partial(kernel, Z, Y, X), out_shape=jax.ShapeDty...  72.7 us
    unnamed x1, local copies, waits for them, and re-layouts  1.57 us

profile of v4, /device:TPU:1, one launch (start us, length us, event | category | flops | bytes accessed | tf_op | source)
XLA Modules:
  0.0 74.9 jit_solution(1241541893823095206)
XLA Ops:
  0.7 72.7 %shard_map.154 = bf16[32,2048]{1,0:T(8,128)(2,1)} custom-call(bf16[32,2048]{1,0:T(8,128)(2,1)} %tokens.1, f32[1,2048]{1,0:T(1,128)} %bitcast.5, bf16[2048,128]{1,0:T(8,128)(2,1)} %w_query.1, bf16[2048,128]{1,0:T(8,128)(2,1)} %w_key.1, bf16[2048,128]{1,0:T(8,128)(2,1)} %w_value.1, bf16[2048,128]{1,0:T(8,128)(2,1)} %w_att_gate.1, bf16[2048,128]{1,0:T(8,128)(2,1)} %w_rec_in.1, ...), custom_call_target="tpu_custom_call" | custom-call | tf_op jit(solution)/shard_map/pallas_call | solution.py:536
  73.3 1.6 %copy.19 = bf16[32,2048]{1,0:T(8,128)(2,1)} copy(bf16[32,2048]{1,0:T(8,128)(2,1)} %shard_map.154) | data formatting | bytes 262144
